TPU v7x, 32 devices: a whole 2x2x4 slice. The times are simulated.
32 devices in a mesh: ep: 8 (over z, core), tp: 4 (over y, x).
Axes of the slice: x: 2, y: 2, z: 4, core: 2. Of those that a mesh axis runs over, the one named last changes fastest.
Arguments:
- resid: bfloat16 [32, 2048], P('ep', 'tp'), may hold values from -6 to 6
- cache_key: bfloat16 [32, 8, 224, 256], P(('ep', 'tp')), may hold values from -360 to 360
- cache_value: bfloat16 [32, 8, 224, 256], P(('ep', 'tp')), may hold values from -6 to 6
- lengths: int32 [32], P(('ep', 'tp')), may hold values from 28 to 224
- lambdas: float32 [8], replicated, may hold values from 0.3 to 0.8
- mix_gain: float32 [2048], replicated, may hold values from 0.1 to 1.9
- query_gain: float32 [128], replicated, may hold values from 0.1 to 1.9
- key_gain: float32 [128], replicated, may hold values from 0.1 to 1.9
- sub_gain: float32 [256], replicated, may hold values from 0.1 to 1.9
- ffn_gain: float32 [2048], replicated, may hold values from 0.1 to 1.9
- w_query: bfloat16 [2048, 2048], P(None, 'tp'), may hold values from -0.125 to 0.125
- w_key: bfloat16 [2048, 2048], P(None, 'tp'), may hold values from -0.125 to 0.125
- w_value: bfloat16 [2048, 2048], P(None, 'tp'), may hold values from -0.125 to 0.125
- w_out: bfloat16 [2048, 2048], P(None, 'tp'), may hold values from -0.125 to 0.125
- routes: int32 [32, 2], P('ep'), may hold values from 0 to 7, all different within a row; in each aligned block of 4 rows (0 to 3, 4 to 7, ...) at most 4 rows name the same one
- route_weights: float32 [32, 2], P('ep'), may hold values from 0.2 to 0.8
- w_gate: bfloat16 [8, 2048, 4096], P('ep', None, 'tp'), may hold values from -0.125 to 0.125
- w_up: bfloat16 [8, 2048, 4096], P('ep', None, 'tp'), may hold values from -0.125 to 0.125
- w_down: bfloat16 [8, 4096, 2048], P('ep', 'tp'), may hold values from -0.09375 to 0.09375
Outputs:
- result: bfloat16 [32, 2048], P('ep', 'tp')
- new_key: bfloat16 [32, 8, 256], P(('ep', 'tp'))
- new_value: bfloat16 [32, 8, 256], P(('ep', 'tp'))
Inputs may be any that keep to these rules, and one draw needn't show every extreme that they name: `routes`: within the 4 rows of one index of ep no expert is named more than 4 times, and in some of them one expert is named exactly 4 times; the two experts of a row differ. `lengths`: every sequence has at least two live positions.
All inputs are finite; a program needn't handle non-finite values.
Results may differ from a plain program's by a relative error of at most 0.0099.
Values may be sent and summed in bfloat16 or wider, within the bound.
A program may use at most 64 MiB of HBM per device.

v0:
```python
import math
import jax
import jax.numpy as jnp
from jax import lax
from jax.sharding import PartitionSpec as P

CAP = 4
epsilon = 1e-06
out_factor = 0.2 + 0.6 * math.exp(-0.3)
masked_score = -1e30


def scaled_rows(values, gain):
    wide = values.astype(jnp.float32)
    return wide * lax.rsqrt(jnp.mean(wide * wide, axis=-1, keepdims=True) + epsilon) * gain


def route_tables(routes, route_weights, experts, capacity):
    flat_routes = routes.reshape(-1)
    expert_hit = (flat_routes[:, None] == jnp.arange(experts, dtype=jnp.int32)[None, :]).astype(
        jnp.int32
    )
    before = jnp.cumsum(expert_hit, axis=0) - expert_hit
    slot_index = jnp.sum(before * expert_hit, axis=1)
    slot_hit = (slot_index[:, None] == jnp.arange(capacity, dtype=jnp.int32)[None, :]).astype(
        jnp.float32
    )
    pair_table = expert_hit.astype(jnp.float32)[:, :, None] * slot_hit[:, None, :]
    pair_table = pair_table.reshape(routes.shape[0], 2, experts, capacity)
    dispatch = jnp.sum(pair_table, axis=1)
    combine = jnp.sum(pair_table * route_weights[:, :, None, None], axis=1)
    return (dispatch, combine)


def attend(
    queries,
    key_rows,
    value_rows,
    past_keys,
    past_values,
    live_len,
    lambdas,
    query_gain,
    key_gain,
    sub_gain,
):
    seq_count, kv_heads, cache_len, key_width = past_keys.shape
    head_dim = key_width // 2
    head_count = lambdas.shape[0]
    group_size = head_count // kv_heads
    value_dim = past_values.shape[-1]
    score_scale = head_dim ** (-0.5)
    q_unit = scaled_rows(
        queries.reshape(seq_count, kv_heads, group_size, 2, head_dim), query_gain
    ).astype(jnp.bfloat16)
    new_key = scaled_rows(key_rows.reshape(seq_count, kv_heads, 2, head_dim), key_gain).astype(
        jnp.bfloat16
    )
    new_value = value_rows.reshape(seq_count, kv_heads, value_dim)
    past_split = past_keys.reshape(seq_count, kv_heads, cache_len, 2, head_dim)
    scores = (
        jnp.einsum("sjgmd,sjlmd->sjgml", q_unit, past_split, preferred_element_type=jnp.float32)
        * score_scale
    )
    own_score = (
        jnp.einsum("sjgmd,sjmd->sjgm", q_unit, new_key, preferred_element_type=jnp.float32)
        * score_scale
    )
    live_mask = jnp.arange(cache_len, dtype=jnp.int32)[None, :] < live_len[:, None]
    scores = jnp.where(live_mask[:, None, None, None, :], scores, masked_score)
    peak = jnp.maximum(jnp.max(scores, axis=-1), own_score)
    past_weight = jnp.exp(scores - peak[..., None])
    own_weight = jnp.exp(own_score - peak)
    totals = jnp.sum(past_weight, axis=-1) + own_weight
    past_prob = past_weight / totals[..., None]
    own_prob = own_weight / totals
    mix_lambda = lambdas.reshape(1, kv_heads, group_size, 1)
    past_mix = (past_prob[..., 0, :] - mix_lambda * past_prob[..., 1, :]).astype(jnp.bfloat16)
    own_mix = (own_prob[..., 0] - mix_lambda[..., 0] * own_prob[..., 1]).astype(jnp.bfloat16)
    head_out = jnp.einsum(
        "sjgl,sjlv->sjgv", past_mix, past_values, preferred_element_type=jnp.float32
    )
    head_out = (
        head_out
        + own_mix.astype(jnp.float32)[..., None] * new_value.astype(jnp.float32)[:, :, None, :]
    )
    mixed = (
        (scaled_rows(head_out, sub_gain) * out_factor)
        .astype(jnp.bfloat16)
        .reshape(seq_count, head_count * value_dim)
    )
    return (mixed, new_key.reshape(seq_count, kv_heads, key_width), new_value)


def local(
    resid,
    cache_key,
    cache_value,
    lengths,
    lambdas,
    mix_gain,
    query_gain,
    key_gain,
    sub_gain,
    ffn_gain,
    w_query,
    w_key,
    w_value,
    w_out,
    routes,
    route_weights,
    w_gate,
    w_up,
    w_down,
):
    gathered = lax.all_gather(resid, "tp", axis=1, tiled=True)
    normed = scaled_rows(gathered, mix_gain).astype(jnp.bfloat16)
    query_part = jnp.dot(normed, w_query, preferred_element_type=jnp.float32).astype(jnp.bfloat16)
    key_part = jnp.dot(normed, w_key, preferred_element_type=jnp.float32).astype(jnp.bfloat16)
    value_part = jnp.dot(normed, w_value, preferred_element_type=jnp.float32).astype(jnp.bfloat16)
    queries, key_rows, value_rows = (
        lax.all_to_all(query_part, "tp", split_axis=0, concat_axis=1, tiled=True),
        lax.all_to_all(key_part, "tp", split_axis=0, concat_axis=1, tiled=True),
        lax.all_to_all(value_part, "tp", split_axis=0, concat_axis=1, tiled=True),
    )
    mixed, new_key, new_value = attend(
        queries,
        key_rows,
        value_rows,
        cache_key,
        cache_value,
        lengths,
        lambdas,
        query_gain,
        key_gain,
        sub_gain,
    )
    attn_proj = jnp.dot(
        lax.all_gather(mixed, "tp", axis=0, tiled=True), w_out, preferred_element_type=jnp.float32
    )
    updated = (resid.astype(jnp.float32) + attn_proj).astype(jnp.bfloat16)
    updated_rows = lax.all_gather(updated, "tp", axis=1, tiled=True)
    hidden = scaled_rows(updated_rows, ffn_gain).astype(jnp.bfloat16)
    experts = w_gate.shape[0] * lax.axis_size("ep")
    dispatch, combine = route_tables(routes, route_weights, experts, CAP)
    send = jnp.einsum(
        "gec,gd->ecd", dispatch.astype(jnp.bfloat16), hidden, preferred_element_type=jnp.float32
    ).astype(jnp.bfloat16)
    slots = lax.all_to_all(send, "ep", split_axis=0, concat_axis=0, tiled=True)
    flat_rows = slots.reshape(-1, slots.shape[-1])
    gate_out = jnp.dot(flat_rows, w_gate[0], preferred_element_type=jnp.float32)
    up_out = jnp.dot(flat_rows, w_up[0], preferred_element_type=jnp.float32)
    act = (jax.nn.silu(gate_out) * up_out).astype(jnp.bfloat16)
    down_out = jnp.dot(act, w_down[0], preferred_element_type=jnp.float32)
    partial_value = down_out.reshape(slots.shape[0], slots.shape[1], down_out.shape[-1])
    flat_combine = combine.reshape(combine.shape[0], -1)
    summed = lax.psum_scatter(
        partial_value.astype(jnp.bfloat16), "tp", scatter_dimension=2, tiled=True
    ).astype(jnp.float32)
    returned = lax.all_to_all(
        summed.astype(jnp.bfloat16), "ep", split_axis=0, concat_axis=0, tiled=True
    ).astype(summed.dtype)
    expert_mix = jnp.dot(
        flat_combine,
        returned.reshape(-1, returned.shape[-1]),
        precision=lax.Precision.HIGHEST,
        preferred_element_type=jnp.float32,
    )
    result = (updated.astype(jnp.float32) + expert_mix).astype(jnp.bfloat16)
    return (result, new_key, new_value)


def solution(mesh):
    in_specs = (
        P("ep", "tp"),
        P(("ep", "tp"), None, None, None),
        P(("ep", "tp"), None, None, None),
        P(("ep", "tp")),
        P(),
        P(),
        P(),
        P(),
        P(),
        P(),
        P(None, "tp"),
        P(None, "tp"),
        P(None, "tp"),
        P(None, "tp"),
        P("ep", None),
        P("ep", None),
        P("ep", None, "tp"),
        P("ep", None, "tp"),
        P("ep", "tp", None),
    )
    out_specs = (P("ep", "tp"), P(("ep", "tp"), None, None), P(("ep", "tp"), None, None))
    return jax.shard_map(local, mesh=mesh, in_specs=in_specs, out_specs=out_specs, check_vma=False)
```

profile of v0, /device:TPU:0, one launch (start us, length us, event | category | flops | bytes accessed | tf_op | source)
XLA Modules:
  0.0 129.9 jit_solution(2296652605895860037)
XLA Ops:
  7.2 0.0 copy-start
  7.2 0.0 copy-start.3
  7.2 9.9 %all_gather.9 = bf16[4,2048]{1,0:T(4,128)(2,1)S(1)} all-gather(bf16[4,512]{1,0:T(4,128)(2,1)} %param.19), channel_id=1, replica_groups=mesh['ep'=8,'tp'=4] {'tp'}, dimensions={1}, use_global_device_ids=true | all-gather | bytes 20480 | tf_op jit(solution)/shard_map/all_gather | solution.py:116
  17.1 0.1 fusion.26
  17.3 1.1 fusion.18
  18.4 0.5 broadcast.214
  18.9 0.7 reduce.19
  19.6 0.6 reshape.382
  20.2 3.2 %all-to-all-start = ((bf16[4,2,256]{2,1,0:T(2,128)(2,1)}), bf16[4,2,256]{2,1,0:T(2,128)(2,1)S(1)}, u32[]{:S(2)}, u32[]{:S(2)}) async-start(bf16[4,2,256]{2,1,0:T(2,128)(2,1)} %reshape.382), calls=%async_computation | async-start | bytes 8192 | tf_op jit(solution)/shard_map/all_to_all | solution.py:122
  23.4 0.1 copy.64
  23.5 0.1 eq.47
  23.6 0.1 fusion.48
  23.7 2.1 %fusion.19 = bf16[4,1,512]{2,0,1:T(4,128)(2,1)S(1)} fusion(bf16[2048,512]{1,0:T(8,128)(2,1)} %param.30, bf16[4,2048]{1,0:T(4,128)(2,1)S(1)} %all_gather.9, f32[2048]{0:T(1024)S(1)} %copy-done.3, f32[4]{0:T(128)S(1)} %add_rsqrt_fusion.4), kind=kOutput, calls=%fused_computation.19 | convolution fusion | flops 8423424 | bytes 2125840 | tf_op jit(solution)/shard_map/dot_general | solution.py:119
  26.5 0.0 copy-start.10
  26.5 0.4 fusion.20
  27.0 0.1 fusion.51
  27.1 0.2 select_reduce_fusion
  27.2 0.1 eq.51
  27.3 0.1 compare_convert_fusion
  27.4 0.1 copy.66
  27.5 0.1 multiply_reduce_fusion
  27.6 0.7 reduce.18
  28.3 0.6 reshape.384
  28.9 2.2 %reshape.356 = bf16[8,224,2,128]{3,2,1,0:T(2,128)(2,1)S(1)} reshape(bf16[1,8,224,256]{3,2,1,0:T(8,128)(2,1)} %param.20) | data formatting | bytes 1835008 | tf_op jit(solution)/shard_map/reshape.7
  31.1 0.7 reduce.17
  31.7 0.6 reshape.380
  32.3 4.2 %all-to-all-start.1 = ((bf16[4,2,256]{2,1,0:T(2,128)(2,1)}), bf16[4,2,256]{2,1,0:T(2,128)(2,1)S(1)}, u32[]{:S(2)}, u32[]{:S(2)}) async-start(bf16[4,2,256]{2,1,0:T(2,128)(2,1)} %reshape.384), calls=%async_computation.1 | async-start | bytes 8192 | tf_op jit(solution)/shard_map/all_to_all | solution.py:123
  36.5 4.6 %all-to-all-done.1 = bf16[4,2,256]{2,1,0:T(2,128)(2,1)S(1)} async-done(((bf16[4,2,256]{2,1,0:T(2,128)(2,1)}), bf16[4,2,256]{2,1,0:T(2,128)(2,1)S(1)}, u32[]{:S(2)}, u32[]{:S(2)}) %all-to-all-start.1) | async-done | bytes 4128 | tf_op jit(solution)/shard_map/all_to_all | solution.py:123
  41.2 3.2 %all-to-all-start.2 = ((bf16[4,2,256]{2,1,0:T(2,128)(2,1)}), bf16[4,2,256]{2,1,0:T(2,128)(2,1)S(1)}, u32[]{:S(2)}, u32[]{:S(2)}) async-start(bf16[4,2,256]{2,1,0:T(2,128)(2,1)} %reshape.380), calls=%async_computation.2 | async-start | bytes 8192 | tf_op jit(solution)/shard_map/all_to_all | solution.py:124
  44.4 0.0 reduce-scatter.2.cloned.1.call-start
  44.6 0.1 reduce_sum.83
  44.6 0.1 reduce_sum.82
  44.8 0.2 fusion.45
  44.9 0.1 copy.79
  45.0 0.6 fusion.23
  45.6 0.1 fusion.41
  45.7 0.2 fusion.40
  45.9 0.1 divide_bitcast_fusion
  46.0 0.1 fusion.49
  46.1 3.0 %all-to-all-done.2 = bf16[4,2,256]{2,1,0:T(2,128)(2,1)S(1)} async-done(((bf16[4,2,256]{2,1,0:T(2,128)(2,1)}), bf16[4,2,256]{2,1,0:T(2,128)(2,1)S(1)}, u32[]{:S(2)}, u32[]{:S(2)}) %all-to-all-start.2) | async-done | bytes 4128 | tf_op jit(solution)/shard_map/all_to_all | solution.py:124
  49.1 1.4 %fusion.21 = f32[8,1,256]{2,1,0:T(1,128)S(1)} fusion(bf16[1,8,224,256]{3,2,1,0:T(8,128)(2,1)} %param.21, bf16[8,224,1]{1,0,2:T(8,128)(2,1)S(1)} %fusion.49), kind=kOutput, calls=%fused_computation.21 | convolution fusion | flops 917504 | bytes 929280 | tf_op jit(solution)/shard_map/sjgl,sjlv->sjgv/dot_general | solution.py:80
  50.5 0.2 multiply_reduce_fusion.1
  50.8 0.1 multiply_convert_fusion.1
  50.8 7.2 %all-gather = bf16[4,1,2048]{2,1,0:T(2,128)(2,1)S(1)} all-gather(bf16[1,1,2048]{2,1,0:T(2,128)(2,1)S(1)} %reshape.365), channel_id=1, replica_groups=mesh['ep'=8,'tp'=4] {'tp'}, dimensions={0}, use_global_device_ids=true | all-gather | bytes 20480 | tf_op jit(solution)/shard_map/all_gather | solution.py:139
  58.1 2.0 %fusion.15 = bf16[4,512]{1,0:T(4,128)(2,1)S(1)} fusion(bf16[2048,512]{1,0:T(8,128)(2,1)} %param.32, bf16[4,1,2048]{2,1,0:T(2,128)(2,1)S(1)} %all-gather, bf16[4,512]{1,0:T(4,128)(2,1)S(1)} %copy-done.4), kind=kOutput, calls=%fused_computation.12 | convolution fusion | flops 8394752 | bytes 2121728 | tf_op jit(solution)/shard_map/dot_general | solution.py:138
  60.1 8.1 %all_gather.11 = bf16[4,2048]{1,0:T(4,128)(2,1)S(1)} all-gather(bf16[4,512]{1,0:T(4,128)(2,1)S(1)} %fusion.15), channel_id=1, replica_groups=mesh['ep'=8,'tp'=4] {'tp'}, dimensions={1}, use_global_device_ids=true | all-gather | bytes 20480 | tf_op jit(solution)/shard_map/all_gather | solution.py:142
  68.2 0.1 fusion.29
  68.3 0.2 convolution_convert_fusion
  68.6 0.1 copy.68
  68.7 11.4 %all_to_all.49 = bf16[8,4,2048]{2,1,0:T(4,128)(2,1)S(1)} all-to-all(bf16[8,4,2048]{2,1,0:T(4,128)(2,1)S(1)} %copy.68), channel_id=1, replica_groups=mesh['ep'=8,'tp'=4] {'ep'}, dimensions={0} | all-to-all | bytes 262144 | tf_op jit(solution)/shard_map/all_to_all | solution.py:149
  80.2 3.2 %fusion.4 = f32[32,1024]{1,0:T(8,128)S(1)} fusion(bf16[32,2048]{1,0:T(8,128)(2,1)S(1)} %reshape.359, bf16[1,2048,1024]{2,1,0:T(8,128)(2,1)} %param.35), kind=kOutput, calls=%fused_computation.4 | convolution fusion | flops 134217728 | bytes 4456448 | tf_op jit(solution)/shard_map/dot_general | solution.py:151
  83.3 0.3 copy-done.1
  83.6 0.8 fusion.12
  84.5 3.6 %fusion.6 = bf16[8,4,2048]{2,0,1:T(8,128)(2,1)} fusion(bf16[1,1024,2048]{2,1,0:T(8,128)(2,1)} %param.37, bf16[8,4,1024]{2,1,0:T(4,128)(2,1)S(1)} %dot_general.48), kind=kOutput, calls=%fused_computation.6 | convolution fusion | flops 134283264 | bytes 4390912 | tf_op jit(solution)/shard_map/dot_general | solution.py:154
  88.1 0.0 reduce-scatter.2.cloned.1.call-update
  88.1 0.1 copy.82
  88.2 0.1 mul.249
  88.3 22.2 %reduce-scatter.2.cloned.1.call-done = bf16[8,4,512]{2,0,1:T(8,128)(2,1)} async-done(((bf16[8,4,2048]{2,0,1:T(8,128)(2,1)}), bf16[8,4,512]{2,0,1:T(8,128)(2,1)}) %reduce-scatter.2.cloned.1.call-update) | async-done | bytes 32784 | tf_op jit(solution)/shard_map/reduce_scatter | solution.py:157
  110.5 1.4 %copy.70 = bf16[8,4,512]{2,1,0:T(4,128)(2,1)} copy(bf16[8,4,512]{2,0,1:T(8,128)(2,1)} %reduce-scatter.2.cloned.1.call-done) | data formatting | bytes 65536 | tf_op jit(solution)/shard_map/reduce_scatter | solution.py:157
  111.9 4.6 %all-to-all-start.4 = ((bf16[8,4,512]{2,1,0:T(4,128)(2,1)}), bf16[8,4,512]{2,1,0:T(4,128)(2,1)S(1)}, u32[]{:S(2)}, u32[]{:S(2)}) async-start(bf16[8,4,512]{2,1,0:T(4,128)(2,1)} %copy.70), calls=%async_computation.5 | async-start | bytes 65536 | tf_op jit(solution)/shard_map/all_to_all | solution.py:160
  116.5 0.6 multiply_convert_fusion
  117.1 0.6 reshape.360
  117.7 4.5 %all-to-all-done.4 = bf16[8,4,512]{2,1,0:T(4,128)(2,1)S(1)} async-done(((bf16[8,4,512]{2,1,0:T(4,128)(2,1)}), bf16[8,4,512]{2,1,0:T(4,128)(2,1)S(1)}, u32[]{:S(2)}, u32[]{:S(2)}) %all-to-all-start.4) | async-done | bytes 32800 | tf_op jit(solution)/shard_map/all_to_all | solution.py:160
  122.2 0.8 fusion.17
  (46 shorter events, 0.4 us)
Async XLA Ops:
  7.2 10.1 %copy-start = (bf16[2048,512]{1,0:T(8,128)(2,1)S(1)}, bf16[2048,512]{1,0:T(8,128)(2,1)}, u32[]{:S(2)}) copy-start(bf16[2048,512]{1,0:T(8,128)(2,1)} %param.29) | copy-start | bytes 6291460
  7.2 16.5 %copy-start.3 = (f32[2048]{0:T(1024)S(1)}, f32[2048]{0:T(1024)}, u32[]{:S(2)}) copy-start(f32[2048]{0:T(1024)} %param.24) | copy-start | bytes 24580
  7.2 16.2 %copy-start.7 = (s32[4,2]{0,1:T(2,128)S(1)}, s32[4,2]{0,1:T(2,128)}, u32[]{:S(2)}) copy-start(s32[4,2]{0,1:T(2,128)} %param.33) | copy-start | bytes 100
  20.2 12.2 %all-to-all-start = ((bf16[4,2,256]{2,1,0:T(2,128)(2,1)}), bf16[4,2,256]{2,1,0:T(2,128)(2,1)S(1)}, u32[]{:S(2)}, u32[]{:S(2)}) async-start(bf16[4,2,256]{2,1,0:T(2,128)(2,1)} %reshape.382), calls=%async_computation | async-start | bytes 8192 | tf_op jit(solution)/shard_map/all_to_all | solution.py:122
  23.6 2.9 %copy-start.2 = (bf16[2048,512]{1,0:T(8,128)(2,1)S(1)}, bf16[2048,512]{1,0:T(8,128)(2,1)}, u32[]{:S(2)}) copy-start(bf16[2048,512]{1,0:T(8,128)(2,1)} %param.31) | copy-start | bytes 6291460
  23.7 3.7 %copy-start.8 = (f32[4,2]{0,1:T(2,128)S(1)}, f32[4,2]{0,1:T(2,128)}, u32[]{:S(2)}) copy-start(f32[4,2]{0,1:T(2,128)} %param.34) | copy-start | bytes 100
  26.5 18.2 %copy-start.10 = (f32[128]{0:T(128)S(1)}, f32[128]{0:T(128)}, u32[]{:S(2)}) copy-start(f32[128]{0:T(128)} %param.25) | copy-start | bytes 1540
  26.5 18.2 %copy-start.11 = (f32[128]{0:T(128)S(1)}, f32[128]{0:T(128)}, u32[]{:S(2)}) copy-start(f32[128]{0:T(128)} %param.26) | copy-start | bytes 1540
  27.0 19.0 %copy-start.6 = (f32[8]{0:T(128)S(1)}, f32[8]{0:T(128)}, u32[]{:S(2)}) copy-start(f32[8]{0:T(128)} %param.23) | copy-start | bytes 100
  27.0 23.8 %copy-start.9 = (f32[256]{0:T(256)S(1)}, f32[256]{0:T(256)}, u32[]{:S(2)}) copy-start(f32[256]{0:T(256)} %param.27) | copy-start | bytes 3076
  28.9 29.2 %copy-start.4 = (bf16[4,512]{1,0:T(4,128)(2,1)S(1)}, bf16[4,512]{1,0:T(4,128)(2,1)}, u32[]{:S(2)}) copy-start(bf16[4,512]{1,0:T(4,128)(2,1)} %param.19) | copy-start | bytes 12292
  32.3 8.8 %all-to-all-start.1 = ((bf16[4,2,256]{2,1,0:T(2,128)(2,1)}), bf16[4,2,256]{2,1,0:T(2,128)(2,1)S(1)}, u32[]{:S(2)}, u32[]{:S(2)}) async-start(bf16[4,2,256]{2,1,0:T(2,128)(2,1)} %reshape.384), calls=%async_computation.1 | async-start | bytes 8192 | tf_op jit(solution)/shard_map/all_to_all | solution.py:123
  41.2 7.9 %all-to-all-start.2 = ((bf16[4,2,256]{2,1,0:T(2,128)(2,1)}), bf16[4,2,256]{2,1,0:T(2,128)(2,1)S(1)}, u32[]{:S(2)}, u32[]{:S(2)}) async-start(bf16[4,2,256]{2,1,0:T(2,128)(2,1)} %reshape.380), calls=%async_computation.2 | async-start | bytes 8192 | tf_op jit(solution)/shard_map/all_to_all | solution.py:124
  44.4 66.1 %reduce-scatter.2.cloned.1.call-start = ((), (), s32[]{:S(2)}) async-start(), calls=%async_computation.6 | async-start | bytes 163840 | tf_op jit(solution)/shard_map/reduce_scatter | solution.py:157
  45.0 23.3 %copy-start.5 = (f32[2048]{0:T(1024)S(1)}, f32[2048]{0:T(1024)}, u32[]{:S(2)}) copy-start(f32[2048]{0:T(1024)} %param.28) | copy-start | bytes 24580
  80.2 3.5 %copy-start.1 = (bf16[1,2048,1024]{2,1,0:T(8,128)(2,1)S(1)}, bf16[1,2048,1024]{2,1,0:T(8,128)(2,1)}, u32[]{:S(2)}) copy-start(bf16[1,2048,1024]{2,1,0:T(8,128)(2,1)} %param.36) | copy-start | bytes 12582916
  111.9 10.3 %all-to-all-start.4 = ((bf16[8,4,512]{2,1,0:T(4,128)(2,1)}), bf16[8,4,512]{2,1,0:T(4,128)(2,1)S(1)}, u32[]{:S(2)}, u32[]{:S(2)}) async-start(bf16[8,4,512]{2,1,0:T(4,128)(2,1)} %copy.70), calls=%async_computation.5 | async-start | bytes 65536 | tf_op jit(solution)/shard_map/all_to_all | solution.py:160
Sparse Core Ops, SparseCore 0:
  88.2 22.2 reduce-scatter.1
where the time goes:
time: 131 us; the launch traced here: 130 us
  blocking collectives  36.7 us (28%)
  waiting for transfers between devices  34.4 us (26%)
  matrix products  16.3 us (12%)
  starting transfers between devices  15.3 us (12%)
  between operations  15 us (11%)
  local copies, waits for them, and re-layouts  7.69 us (6%)
  other arithmetic  4.59 us (4%)
    reduce_scatter x1, waiting for transfers between devices, local(): lax.psum_scatter(partial_value.astype(jnp.bfloat16), 'tp', scatter_dimens...  22.2 us
    all_to_all x1, blocking collectives, local(): slots = lax.all_to_all(send, 'ep', split_axis=0, concat_axis=0, tiled=True)  11.4 us
    all_gather x1, blocking collectives, local(): gathered = lax.all_gather(resid, 'tp', axis=1, tiled=True)  9.93 us
    all_gather x1, blocking collectives, local(): updated_rows = lax.all_gather(updated, 'tp', axis=1, tiled=True)  8.12 us
    all_gather x1, blocking collectives, local(): lax.all_gather(mixed, 'tp', axis=0, tiled=True)  7.25 us
    all_to_all x1, waiting for transfers between devices, local(): lax.all_to_all(key_part, 'tp', split_axis=0, concat_axis=1, tiled=True)  4.63 us
    all_to_all x1, starting transfers between devices, local(): lax.all_to_all(summed.astype(jnp.bfloat16), 'ep', split_axis=0, concat_ax...  4.6 us
    all_to_all x1, waiting for transfers between devices, local(): lax.all_to_all(summed.astype(jnp.bfloat16), 'ep', split_axis=0, concat_ax...  4.51 us
  transfers between devices with their start and end apart: 5, of which 4 were waited for; matrix products, arithmetic and copies ran while one was open for 9% of the time, Pallas kernels for 0%

commit v1 on v0

--- a/solution.py
+++ b/solution.py
@@ -113,7 +113,7 @@
     w_up,
     w_down,
 ):
-    gathered = lax.all_gather(resid, "tp", axis=1, tiled=True)
+    gathered = jnp.concatenate(lax.all_gather(resid, "tp"), axis=1)
     normed = scaled_rows(gathered, mix_gain).astype(jnp.bfloat16)
     query_part = jnp.dot(normed, w_query, preferred_element_type=jnp.float32).astype(jnp.bfloat16)
     key_part = jnp.dot(normed, w_key, preferred_element_type=jnp.float32).astype(jnp.bfloat16)

time: 131 us -> 131 us (level)
    all_to_all x1, waiting for transfers between devices: 4.63 us -> 0.01 us  [local(): lax.all_to_all(key_part, 'tp', split_axis=0, concat_axis=1, tiled=True)]
    all_to_all x1, waiting for transfers between devices: 0.01 us -> 4.61 us  [local(): lax.all_to_all(query_part, 'tp', split_axis=0, concat_axis=1, tiled=True)]
    dot_general x1, matrix products: 2.14 us -> 0.37 us  [local(): jnp.dot(normed, w_key, preferred_element_type=jnp.float32)]
  transfers between devices with their start and end apart: 5 -> 5, of which waited for: 4 -> 4; matrix products, arithmetic and copies ran while one was open for 9% -> 8% of each run, Pallas kernels for 0% -> 0%
where the time goes in v1:
time: 131 us; the launch traced here: 130 us
  blocking collectives  36.7 us (28%)
  waiting for transfers between devices  34.4 us (26%)
  matrix products  15.4 us (12%)
  starting transfers between devices  15.3 us (12%)
  between operations  15 us (11%)
  local copies, waits for them, and re-layouts  7.69 us (6%)
  other arithmetic  5.37 us (4%)
    reduce_scatter x1, waiting for transfers between devices, local(): lax.psum_scatter(partial_value.astype(jnp.bfloat16), 'tp', scatter_dimens...  22.2 us
    all_to_all x1, blocking collectives, local(): slots = lax.all_to_all(send, 'ep', split_axis=0, concat_axis=0, tiled=True)  11.4 us
    all_gather x1, blocking collectives, local(): gathered = jnp.concatenate(lax.all_gather(resid, 'tp'), axis=1)  9.93 us
    all_gather x1, blocking collectives, local(): updated_rows = lax.all_gather(updated, 'tp', axis=1, tiled=True)  8.12 us
    all_gather x1, blocking collectives, local(): lax.all_gather(mixed, 'tp', axis=0, tiled=True)  7.25 us
    all_to_all x1, waiting for transfers between devices, local(): lax.all_to_all(query_part, 'tp', split_axis=0, concat_axis=1, tiled=True)  4.61 us
    all_to_all x1, starting transfers between devices, local(): lax.all_to_all(summed.astype(jnp.bfloat16), 'ep', split_axis=0, concat_ax...  4.6 us
    all_to_all x1, waiting for transfers between devices, local(): lax.all_to_all(summed.astype(jnp.bfloat16), 'ep', split_axis=0, concat_ax...  4.51 us
  transfers between devices with their start and end apart: 5, of which 4 were waited for; matrix products, arithmetic and copies ran while one was open for 8% of the time, Pallas kernels for 0%

profile of v1, /device:TPU:0, one launch (start us, length us, event | category | flops | bytes accessed | tf_op | source)
XLA Modules:
  0.0 129.9 jit_solution(7970023615273310814)
XLA Ops:
  7.2 0.0 copy-start
  7.2 9.9 %all-gather.1 = bf16[4,4,512]{2,1,0:T(4,128)(2,1)S(1)} all-gather(bf16[1,4,512]{2,1,0:T(4,128)(2,1)} %bitcast.117), channel_id=2, replica_groups=mesh['ep'=8,'tp'=4] {'tp'}, dimensions={0}, use_global_device_ids=true | all-gather | bytes 20480 | tf_op jit(solution)/shard_map/all_gather | solution.py:116
  17.1 0.1 multiply_reduce_fusion
  17.3 0.8 multiply_convert_fusion
  18.1 0.4 fusion.19
  18.4 0.5 broadcast.214
  19.0 0.7 reduce.20
  19.6 0.6 reshape.396
  20.2 3.2 %all-to-all-start.1 = ((bf16[4,2,256]{2,1,0:T(2,128)(2,1)}), bf16[4,2,256]{2,1,0:T(2,128)(2,1)S(1)}, u32[]{:S(2)}, u32[]{:S(2)}) async-start(bf16[4,2,256]{2,1,0:T(2,128)(2,1)} %reshape.396), calls=%async_computation.1 | async-start | bytes 8192 | tf_op jit(solution)/shard_map/all_to_all | solution.py:123
  23.5 0.1 copy.64
  23.6 0.1 eq.47
  23.7 0.1 fusion.45
  23.7 2.1 %fusion.18 = bf16[4,1,512]{2,0,1:T(4,128)(2,1)S(1)} fusion(bf16[4,2048]{1,0:T(4,128)(2,1)S(1)} %multiply_convert_fusion, bf16[2048,512]{1,0:T(8,128)(2,1)} %param.29), kind=kOutput, calls=%fused_computation.18 | convolution fusion | flops 8390656 | bytes 2117632 | tf_op jit(solution)/shard_map/dot_general | solution.py:118
  26.5 0.0 copy-start.9
  26.5 0.4 fusion.20
  26.9 0.1 fusion.48
  27.0 0.2 select_reduce_fusion
  27.2 0.1 eq.51
  27.3 0.1 compare_convert_fusion
  27.4 0.1 copy.66
  27.5 0.1 multiply_reduce_fusion.1
  27.6 0.7 reduce.21
  28.3 0.6 reshape.394
  28.9 2.2 %reshape.360 = bf16[8,224,2,128]{3,2,1,0:T(2,128)(2,1)S(1)} reshape(bf16[1,8,224,256]{3,2,1,0:T(8,128)(2,1)} %param.20) | data formatting | bytes 1835008 | tf_op jit(solution)/shard_map/reshape.7
  31.0 0.7 reduce.19
  31.7 0.6 reshape.392
  32.3 4.2 %all-to-all-start = ((bf16[4,2,256]{2,1,0:T(2,128)(2,1)}), bf16[4,2,256]{2,1,0:T(2,128)(2,1)S(1)}, u32[]{:S(2)}, u32[]{:S(2)}) async-start(bf16[4,2,256]{2,1,0:T(2,128)(2,1)} %reshape.394), calls=%async_computation | async-start | bytes 8192 | tf_op jit(solution)/shard_map/all_to_all | solution.py:122
  36.5 4.6 %all-to-all-done = bf16[4,2,256]{2,1,0:T(2,128)(2,1)S(1)} async-done(((bf16[4,2,256]{2,1,0:T(2,128)(2,1)}), bf16[4,2,256]{2,1,0:T(2,128)(2,1)S(1)}, u32[]{:S(2)}, u32[]{:S(2)}) %all-to-all-start) | async-done | bytes 4128 | tf_op jit(solution)/shard_map/all_to_all | solution.py:122
  41.1 3.2 %all-to-all-start.2 = ((bf16[4,2,256]{2,1,0:T(2,128)(2,1)}), bf16[4,2,256]{2,1,0:T(2,128)(2,1)S(1)}, u32[]{:S(2)}, u32[]{:S(2)}) async-start(bf16[4,2,256]{2,1,0:T(2,128)(2,1)} %reshape.392), calls=%async_computation.2 | async-start | bytes 8192 | tf_op jit(solution)/shard_map/all_to_all | solution.py:124
  44.4 0.0 reduce-scatter.2.cloned.1.call-start
  44.5 0.1 reduce_sum.83
  44.6 0.1 reduce_sum.82
  44.7 0.2 fusion.42
  44.9 0.1 copy.79
  45.0 0.6 fusion.23
  45.5 0.1 fusion.38
  45.6 0.2 fusion.37
  45.8 0.1 divide_bitcast_fusion
  45.9 0.1 fusion.46
  46.0 3.0 %all-to-all-done.2 = bf16[4,2,256]{2,1,0:T(2,128)(2,1)S(1)} async-done(((bf16[4,2,256]{2,1,0:T(2,128)(2,1)}), bf16[4,2,256]{2,1,0:T(2,128)(2,1)S(1)}, u32[]{:S(2)}, u32[]{:S(2)}) %all-to-all-start.2) | async-done | bytes 4128 | tf_op jit(solution)/shard_map/all_to_all | solution.py:124
  49.1 1.4 %fusion.21 = f32[8,1,256]{2,1,0:T(1,128)S(1)} fusion(bf16[1,8,224,256]{3,2,1,0:T(8,128)(2,1)} %param.21, bf16[8,224,1]{1,0,2:T(8,128)(2,1)S(1)} %fusion.46), kind=kOutput, calls=%fused_computation.21 | convolution fusion | flops 917504 | bytes 929280 | tf_op jit(solution)/shard_map/sjgl,sjlv->sjgv/dot_general | solution.py:80
  50.5 0.2 multiply_reduce_fusion.2
  50.7 0.1 multiply_convert_fusion.2
  50.8 7.2 %all-gather.2 = bf16[4,1,2048]{2,1,0:T(2,128)(2,1)S(1)} all-gather(bf16[1,1,2048]{2,1,0:T(2,128)(2,1)S(1)} %reshape.375), channel_id=1, replica_groups=mesh['ep'=8,'tp'=4] {'tp'}, dimensions={0}, use_global_device_ids=true | all-gather | bytes 20480 | tf_op jit(solution)/shard_map/all_gather | solution.py:139
  58.1 2.0 %fusion.15 = bf16[4,512]{1,0:T(4,128)(2,1)S(1)} fusion(bf16[2048,512]{1,0:T(8,128)(2,1)} %param.32, bf16[4,1,2048]{2,1,0:T(2,128)(2,1)S(1)} %all-gather.2, bf16[4,512]{1,0:T(4,128)(2,1)S(1)} %copy-done.3), kind=kOutput, calls=%fused_computation.12 | convolution fusion | flops 8394752 | bytes 2121728 | tf_op jit(solution)/shard_map/dot_general | solution.py:138
  60.0 8.1 %all_gather.15 = bf16[4,2048]{1,0:T(4,128)(2,1)S(1)} all-gather(bf16[4,512]{1,0:T(4,128)(2,1)S(1)} %fusion.15), channel_id=1, replica_groups=mesh['ep'=8,'tp'=4] {'tp'}, dimensions={1}, use_global_device_ids=true | all-gather | bytes 20480 | tf_op jit(solution)/shard_map/all_gather | solution.py:142
  68.2 0.1 fusion.26
  68.3 0.2 convolution_convert_fusion
  68.5 0.1 copy.68
  68.7 11.4 %all_to_all.49 = bf16[8,4,2048]{2,1,0:T(4,128)(2,1)S(1)} all-to-all(bf16[8,4,2048]{2,1,0:T(4,128)(2,1)S(1)} %copy.68), channel_id=1, replica_groups=mesh['ep'=8,'tp'=4] {'ep'}, dimensions={0} | all-to-all | bytes 262144 | tf_op jit(solution)/shard_map/all_to_all | solution.py:149
  80.1 3.2 %fusion.4 = f32[32,1024]{1,0:T(8,128)S(1)} fusion(bf16[32,2048]{1,0:T(8,128)(2,1)S(1)} %reshape.363, bf16[1,2048,1024]{2,1,0:T(8,128)(2,1)} %param.35), kind=kOutput, calls=%fused_computation.4 | convolution fusion | flops 134217728 | bytes 4456448 | tf_op jit(solution)/shard_map/dot_general | solution.py:151
  83.3 0.3 copy-done.1
  83.6 0.8 fusion.12
  84.4 3.6 %fusion.6 = bf16[8,4,2048]{2,0,1:T(8,128)(2,1)} fusion(bf16[1,1024,2048]{2,1,0:T(8,128)(2,1)} %param.37, bf16[8,4,1024]{2,1,0:T(4,128)(2,1)S(1)} %dot_general.48), kind=kOutput, calls=%fused_computation.6 | convolution fusion | flops 134283264 | bytes 4390912 | tf_op jit(solution)/shard_map/dot_general | solution.py:154
  88.1 0.0 reduce-scatter.2.cloned.1.call-update
  88.1 0.1 copy.82
  88.2 0.1 mul.251
  88.3 22.2 %reduce-scatter.2.cloned.1.call-done = bf16[8,4,512]{2,0,1:T(8,128)(2,1)} async-done(((bf16[8,4,2048]{2,0,1:T(8,128)(2,1)}), bf16[8,4,512]{2,0,1:T(8,128)(2,1)}) %reduce-scatter.2.cloned.1.call-update) | async-done | bytes 32784 | tf_op jit(solution)/shard_map/reduce_scatter | solution.py:157
  110.5 1.4 %copy.70 = bf16[8,4,512]{2,1,0:T(4,128)(2,1)} copy(bf16[8,4,512]{2,0,1:T(8,128)(2,1)} %reduce-scatter.2.cloned.1.call-done) | data formatting | bytes 65536 | tf_op jit(solution)/shard_map/reduce_scatter | solution.py:157
  111.9 4.6 %all-to-all-start.4 = ((bf16[8,4,512]{2,1,0:T(4,128)(2,1)}), bf16[8,4,512]{2,1,0:T(4,128)(2,1)S(1)}, u32[]{:S(2)}, u32[]{:S(2)}) async-start(bf16[8,4,512]{2,1,0:T(4,128)(2,1)} %copy.70), calls=%async_computation.5 | async-start | bytes 65536 | tf_op jit(solution)/shard_map/all_to_all | solution.py:160
  116.5 0.6 multiply_convert_fusion.1
  117.1 0.6 reshape.364
  117.7 4.5 %all-to-all-done.4 = bf16[8,4,512]{2,1,0:T(4,128)(2,1)S(1)} async-done(((bf16[8,4,512]{2,1,0:T(4,128)(2,1)}), bf16[8,4,512]{2,1,0:T(4,128)(2,1)S(1)}, u32[]{:S(2)}, u32[]{:S(2)}) %all-to-all-start.4) | async-done | bytes 32800 | tf_op jit(solution)/shard_map/all_to_all | solution.py:160
  122.2 0.8 fusion.17
  (46 shorter events, 0.4 us)
Async XLA Ops:
  7.2 10.9 %copy-start = (bf16[2048,512]{1,0:T(8,128)(2,1)S(1)}, bf16[2048,512]{1,0:T(8,128)(2,1)}, u32[]{:S(2)}) copy-start(bf16[2048,512]{1,0:T(8,128)(2,1)} %param.30) | copy-start | bytes 6291460
  7.2 16.3 %copy-start.6 = (s32[4,2]{0,1:T(2,128)S(1)}, s32[4,2]{0,1:T(2,128)}, u32[]{:S(2)}) copy-start(s32[4,2]{0,1:T(2,128)} %param.33) | copy-start | bytes 100
  20.2 12.1 %all-to-all-start.1 = ((bf16[4,2,256]{2,1,0:T(2,128)(2,1)}), bf16[4,2,256]{2,1,0:T(2,128)(2,1)S(1)}, u32[]{:S(2)}, u32[]{:S(2)}) async-start(bf16[4,2,256]{2,1,0:T(2,128)(2,1)} %reshape.396), calls=%async_computation.1 | async-start | bytes 8192 | tf_op jit(solution)/shard_map/all_to_all | solution.py:123
  23.7 2.8 %copy-start.2 = (bf16[2048,512]{1,0:T(8,128)(2,1)S(1)}, bf16[2048,512]{1,0:T(8,128)(2,1)}, u32[]{:S(2)}) copy-start(bf16[2048,512]{1,0:T(8,128)(2,1)} %param.31) | copy-start | bytes 6291460
  23.7 3.6 %copy-start.7 = (f32[4,2]{0,1:T(2,128)S(1)}, f32[4,2]{0,1:T(2,128)}, u32[]{:S(2)}) copy-start(f32[4,2]{0,1:T(2,128)} %param.34) | copy-start | bytes 100
  26.5 18.2 %copy-start.9 = (f32[128]{0:T(128)S(1)}, f32[128]{0:T(128)}, u32[]{:S(2)}) copy-start(f32[128]{0:T(128)} %param.25) | copy-start | bytes 1540
  26.5 18.2 %copy-start.10 = (f32[128]{0:T(128)S(1)}, f32[128]{0:T(128)}, u32[]{:S(2)}) copy-start(f32[128]{0:T(128)} %param.26) | copy-start | bytes 1540
  26.9 19.0 %copy-start.5 = (f32[8]{0:T(128)S(1)}, f32[8]{0:T(128)}, u32[]{:S(2)}) copy-start(f32[8]{0:T(128)} %param.23) | copy-start | bytes 100
  26.9 23.8 %copy-start.8 = (f32[256]{0:T(256)S(1)}, f32[256]{0:T(256)}, u32[]{:S(2)}) copy-start(f32[256]{0:T(256)} %param.27) | copy-start | bytes 3076
  28.9 29.2 %copy-start.3 = (bf16[4,512]{1,0:T(4,128)(2,1)S(1)}, bf16[4,512]{1,0:T(4,128)(2,1)}, u32[]{:S(2)}) copy-start(bf16[4,512]{1,0:T(4,128)(2,1)} %param.19) | copy-start | bytes 12292
  32.3 8.8 %all-to-all-start = ((bf16[4,2,256]{2,1,0:T(2,128)(2,1)}), bf16[4,2,256]{2,1,0:T(2,128)(2,1)S(1)}, u32[]{:S(2)}, u32[]{:S(2)}) async-start(bf16[4,2,256]{2,1,0:T(2,128)(2,1)} %reshape.394), calls=%async_computation | async-start | bytes 8192 | tf_op jit(solution)/shard_map/all_to_all | solution.py:122
  41.1 7.9 %all-to-all-start.2 = ((bf16[4,2,256]{2,1,0:T(2,128)(2,1)}), bf16[4,2,256]{2,1,0:T(2,128)(2,1)S(1)}, u32[]{:S(2)}, u32[]{:S(2)}) async-start(bf16[4,2,256]{2,1,0:T(2,128)(2,1)} %reshape.392), calls=%async_computation.2 | async-start | bytes 8192 | tf_op jit(solution)/shard_map/all_to_all | solution.py:124
  44.4 66.1 %reduce-scatter.2.cloned.1.call-start = ((), (), s32[]{:S(2)}) async-start(), calls=%async_computation.6 | async-start | bytes 163840 | tf_op jit(solution)/shard_map/reduce_scatter | solution.py:157
  45.0 23.3 %copy-start.4 = (f32[2048]{0:T(1024)S(1)}, f32[2048]{0:T(1024)}, u32[]{:S(2)}) copy-start(f32[2048]{0:T(1024)} %param.28) | copy-start | bytes 24580
  80.1 3.5 %copy-start.1 = (bf16[1,2048,1024]{2,1,0:T(8,128)(2,1)S(1)}, bf16[1,2048,1024]{2,1,0:T(8,128)(2,1)}, u32[]{:S(2)}) copy-start(bf16[1,2048,1024]{2,1,0:T(8,128)(2,1)} %param.36) | copy-start | bytes 12582916
  111.9 10.3 %all-to-all-start.4 = ((bf16[8,4,512]{2,1,0:T(4,128)(2,1)}), bf16[8,4,512]{2,1,0:T(4,128)(2,1)S(1)}, u32[]{:S(2)}, u32[]{:S(2)}) async-start(bf16[8,4,512]{2,1,0:T(4,128)(2,1)} %copy.70), calls=%async_computation.5 | async-start | bytes 65536 | tf_op jit(solution)/shard_map/all_to_all | solution.py:160
Sparse Core Ops, SparseCore 0:
  88.2 22.2 reduce-scatter.1
